TPU v7x, 32 devices: a whole 2x2x4 slice. The times are simulated.
32 devices in a mesh: grp: 2 (over x), ep: 16 (over z, y, core).
Axes of the slice: x: 2, y: 2, z: 4, core: 2. Of those that a mesh axis runs over, the one named last changes fastest.
Arguments:
- tokens: bfloat16 [256, 2048], P(('grp', 'ep')), parts along dimension 0, may hold values from -24 to 24
- norm_gain: bfloat16 [2048], replicated, may hold values from 0.099609375 to 1.8984375
- w_query: bfloat16 [2048, 512], P('ep'), may hold values from -0.1875 to 0.1875
- w_key: bfloat16 [2048, 128], replicated, may hold values from -0.125 to 0.125
- w_value: bfloat16 [2048, 128], replicated, may hold values from -0.125 to 0.125
- w_out: bfloat16 [512, 2048], P(None, 'ep'), may hold values from -1 to 1
- cache_k: bfloat16 [256, 1024, 128], P(('grp', 'ep')), parts along dimension 0, may hold values from -6 to 6
- cache_v: bfloat16 [256, 1024, 128], P(('grp', 'ep')), parts along dimension 0, may hold values from -6 to 6
- head_offset: float32 [8], replicated, may hold values from -12 to -3
- key_shift: float32 [256, 2, 1024], P(('grp', 'ep')), parts along dimension 0, may hold values from -3 to 9
- lengths: int32 [256], P(('grp', 'ep')), parts along dimension 0, may hold values from 1 to 1024, 65536 in all
- moe_gain: bfloat16 [2048], replicated, may hold values from 0.099609375 to 1.8984375
- route_ids: int32 [256, 6], P(('grp', 'ep')), parts along dimension 0, may hold values from 0 to 15, all different within a row; in each aligned block of 8 rows (0 to 7, 8 to 15, ...) at most 6 rows name the same one
- route_score: float32 [256, 6], P(('grp', 'ep')), parts along dimension 0, may hold values from 0.05 to 1
- w_gate: bfloat16 [16, 2048, 256], P('ep'), may hold values from -0.125 to 0.125
- w_up: bfloat16 [16, 2048, 256], P('ep'), may hold values from -0.125 to 0.125
- w_down: bfloat16 [16, 256, 2048], P('ep'), may hold values from -0.375 to 0.375
- shared_gate: bfloat16 [2048, 256], replicated, may hold values from -0.125 to 0.125
- shared_up: bfloat16 [2048, 256], replicated, may hold values from -0.125 to 0.125
- shared_down: bfloat16 [256, 2048], replicated, may hold values from -0.375 to 0.375
Outputs:
- out: bfloat16 [256, 2048], P(('grp', 'ep')), parts along dimension 0
- new_key: bfloat16 [256, 128], P(('grp', 'ep')), parts along dimension 0
- new_value: bfloat16 [256, 128], P(('grp', 'ep')), parts along dimension 0
There are 2 independent parts, one for each index of `grp`. A program takes and returns all parts, laid end to end along the dimension named above; an argument that names none is the same for every part. Nothing has to cross between parts.
Inputs may be any that keep to these rules, and one draw needn't show every extreme that they name: Each sequence's cache holds lengths[b] past positions at the start; the new token stands at position lengths[b]. Some sequence of every part has exactly 1024. `route_ids`: the 6 experts of a token differ. Among the tokens of one device, no expert is named more than 6 times, a bound that some block reaches in every draw.
All inputs are finite; a program needn't handle non-finite values. No bound on the sum of `lengths` on one device may be relied on, other than what follows from the above.
Results may differ from a plain program's by a relative error of at most 0.0069.
Values may be sent and summed in bfloat16 or wider, within the bound.
A program may use at most 64 MiB of HBM per device.

v0:
```python
import math
import jax
import jax.numpy as jnp
from jax import lax
from jax.sharding import PartitionSpec as P

EPSILON = 1e-06
ROUTED_SCALE = 2.5


def norm_rows(values, gain_vec):
    mean_sq = jnp.mean(values * values, axis=-1, keepdims=True)
    return values * lax.rsqrt(mean_sq + EPSILON) * gain_vec.astype(jnp.float32)


def swiglu(row_block, gate_w, up_w, down_w):
    gate_part = jnp.dot(row_block, gate_w, preferred_element_type=jnp.float32)
    up_part = jnp.dot(row_block, up_w, preferred_element_type=jnp.float32)
    hidden = (jax.nn.silu(gate_part) * up_part).astype(jnp.bfloat16)
    return jnp.dot(hidden, down_w, preferred_element_type=jnp.float32)


def stick_weights(logits, offset, shifts, lengths):
    logits = logits + offset[None, :, :, None] + shifts[:, :, None, :]
    place_destinations = jnp.arange(logits.shape[-1], dtype=jnp.int32)
    is_live = place_destinations[None, None, None, :] < lengths[:, None, None, None]
    log_fall = jnp.where(is_live, jax.nn.log_sigmoid(-logits), 0.0)
    later_sum = lax.cumsum(log_fall, axis=3, reverse=True) - log_fall
    return jnp.where(is_live, jnp.exp(jax.nn.log_sigmoid(logits) + later_sum), 0.0).astype(
        jnp.bfloat16
    )


def attend(queries, cache_k, cache_v, offset, shifts, lengths):
    seq_count, cache_len, kv_width = cache_k.shape
    groups = shifts.shape[1]
    head_dim = kv_width // groups
    per_group = queries.shape[1] // kv_width
    query_heads = queries.reshape(seq_count, groups, per_group, head_dim)
    key_heads = cache_k.reshape(seq_count, cache_len, groups, head_dim)
    value_heads = cache_v.reshape(seq_count, cache_len, groups, head_dim)
    logits = jnp.einsum(
        "sgrd,slgd->sgrl", query_heads, key_heads, preferred_element_type=jnp.float32
    ) / math.sqrt(head_dim)
    weights = stick_weights(logits, offset.reshape(groups, per_group), shifts, lengths)
    mixed_out = jnp.einsum(
        "sgrl,slgd->sgrd", weights, value_heads, preferred_element_type=jnp.float32
    )
    return mixed_out.reshape(seq_count, queries.shape[1]).astype(jnp.bfloat16)


def shards(
    tokens,
    norm_gain,
    w_query,
    w_key,
    w_value,
    w_out,
    cache_k,
    cache_v,
    head_offset,
    key_shift,
    lengths,
    moe_gain,
    route_ids,
    route_score,
    w_gate,
    w_up,
    w_down,
    shared_gate,
    shared_up,
    shared_down,
):
    seq_dev, model_width = tokens.shape
    devices = lax.axis_size("ep")
    normed = norm_rows(tokens.astype(jnp.float32), norm_gain).astype(jnp.bfloat16)
    new_key = jnp.dot(normed, w_key, preferred_element_type=jnp.float32).astype(jnp.bfloat16)
    new_value = jnp.dot(normed, w_value, preferred_element_type=jnp.float32).astype(jnp.bfloat16)
    queries = jnp.dot(
        normed,
        lax.all_gather(w_query, "ep", axis=0, tiled=True),
        preferred_element_type=jnp.float32,
    )
    queries = queries.astype(jnp.bfloat16)
    attended = attend(queries, cache_k, cache_v, head_offset, key_shift, lengths)
    out_columns = jnp.dot(
        lax.all_gather(attended, "ep", axis=0, tiled=True),
        w_out,
        preferred_element_type=jnp.float32,
    ).astype(jnp.bfloat16)
    branch = lax.all_to_all(out_columns, "ep", split_axis=0, concat_axis=1, tiled=True)
    residual = tokens.astype(jnp.float32) + branch.astype(jnp.float32)
    moe_in = norm_rows(residual, moe_gain).astype(jnp.bfloat16)
    route_share = ROUTED_SCALE * route_score / jnp.sum(route_score, axis=1, keepdims=True)
    shared = swiglu(moe_in, shared_gate, shared_up, shared_down)
    local_count = w_gate.shape[0]
    experts_all = local_count * devices
    expert_iota = jnp.arange(experts_all, dtype=jnp.int32)
    top_count = route_ids.shape[1]
    capacity = max(2, 2 * seq_dev * top_count // experts_all)
    flat_ids = route_ids.reshape(-1)
    hit_table = (flat_ids[:, None] == expert_iota[None, :]).astype(jnp.int32)
    before = jnp.cumsum(hit_table, axis=0) - hit_table
    slot_index = jnp.sum(before * hit_table, axis=1)
    slot_place = flat_ids * capacity + slot_index
    slot_iota = jnp.arange(experts_all * capacity, dtype=jnp.int32)
    dispatch = jnp.sum(
        (slot_iota[:, None, None] == slot_place.reshape(seq_dev, top_count)[None, :, :]).astype(
            jnp.int32
        ),
        axis=2,
    ).astype(jnp.bfloat16)
    outgoing = jnp.dot(dispatch, moe_in, preferred_element_type=jnp.float32).astype(jnp.bfloat16)
    outgoing = outgoing.reshape(experts_all, capacity, model_width)
    arrived = lax.all_to_all(outgoing, "ep", split_axis=0, concat_axis=0, tiled=True)
    slot_count = arrived.shape[1]
    grouped = arrived.reshape(devices, local_count, slot_count, model_width)
    gate_part = jnp.einsum("sekd,edf->sekf", grouped, w_gate, preferred_element_type=jnp.float32)
    up_part = jnp.einsum("sekd,edf->sekf", grouped, w_up, preferred_element_type=jnp.float32)
    hidden = (jax.nn.silu(gate_part) * up_part).astype(jnp.bfloat16)
    result = jnp.einsum("sekf,efd->sekd", hidden, w_down, preferred_element_type=jnp.float32)
    result = result.astype(jnp.bfloat16).reshape(devices * local_count, slot_count, model_width)
    returned = lax.all_to_all(result, "ep", split_axis=0, concat_axis=0, tiled=True)
    returned_rows = returned.reshape(experts_all * capacity, model_width)
    picked = jnp.take(returned_rows, slot_place, axis=0).reshape(seq_dev, top_count, model_width)
    routed = jnp.sum(picked.astype(jnp.float32) * route_share[:, :, None], axis=1)
    out = (residual + routed + shared).astype(jnp.bfloat16)
    return (out, new_key, new_value)


def solution(mesh):
    placed = (
        P(("grp", "ep"), None),
        P(),
        P("ep", None),
        P(),
        P(),
        P(None, "ep"),
        P(("grp", "ep"), None, None),
        P(("grp", "ep"), None, None),
        P(),
        P(("grp", "ep"), None, None),
        P(("grp", "ep")),
        P(),
        P(("grp", "ep"), None),
        P(("grp", "ep"), None),
        P("ep", None, None),
        P("ep", None, None),
        P("ep", None, None),
        P(),
        P(),
        P(),
    )
    return jax.shard_map(
        shards,
        mesh=mesh,
        in_specs=placed,
        out_specs=(P(("grp", "ep"), None), P(("grp", "ep"), None), P(("grp", "ep"), None)),
        check_vma=False,
    )
```

profile of v0, /device:TPU:0, one launch (start us, length us, event | category | flops | bytes accessed | tf_op | source)
XLA Modules:
  0.0 228.9 jit_solution(18109210225156370043)
XLA Ops:
  7.2 0.0 copy-start
  7.2 0.0 all-gather.2.cloned.1.call-start
  7.2 0.7 all-gather.2.cloned.1.call-update
  7.9 0.7 convert_element_type.77
  8.6 4.1 %copy.39 = bf16[8,1024,128]{1,2,0:T(8,128)(2,1)} copy(bf16[8,1024,128]{2,1,0:T(8,128)(2,1)} %param.26) | data formatting | bytes 4194304 | tf_op args[6]
  12.7 0.0 copy-done.11
  12.7 0.1 add.102
  12.8 0.0 copy-done.2
  12.8 0.0 copy-start.10
  12.8 2.6 %copy.42 = bf16[8,1024,128]{1,2,0:T(8,128)(2,1)} copy(bf16[8,1024,128]{2,1,0:T(8,128)(2,1)S(1)} %copy-done.2) | data formatting | bytes 4194304 | tf_op args[7]
  15.4 0.0 copy-done.7
  15.4 0.1 reshape.160
  15.5 0.1 fusion.35
  15.6 0.1 reduce_window_sum.27
  15.6 0.2 select_reduce_fusion
  15.8 0.1 reduce_sum.60
  15.9 0.1 copy.43
  16.0 0.0 copy-done.9
  16.0 0.1 fusion.31
  16.2 0.0 copy-done.10
  16.2 0.1 iota_compare_fusion
  16.2 38.1 %all-gather.2.cloned.1.call-done = bf16[2048,512]{1,0:T(8,128)(2,1)} async-done(((bf16[128,512]{1,0:T(8,128)(2,1)}), bf16[2048,512]{1,0:T(8,128)(2,1)}) %all-gather.2.cloned.1.call-update) | async-done | bytes 2097168 | tf_op jit(solution)/shard_map/all_gather | solution.py:81
  54.4 2.0 convolution_convert_fusion.4
  56.4 0.1 reshape.155
  56.5 0.0 copy-start.3
  56.5 3.0 %fusion.22 = (f32[8,2,4,1024]{3,2,1,0:T(4,128)S(1)}, f32[8,2,4,1024]{3,2,1,0:T(4,128)}) fusion(pred[8,1024]{1,0:T(8,128)(4,1)S(1)} %iota_compare_fusion, f32[8,2,1024]{2,1,0:T(2,128)} %param.29, f32[2,4]{1,0:T(2,128)S(1)} %add.102, bf16[8,2,4,64]{3,2,1,0:T(4,128)(2,1)S(1)} %reshape.155, bf16[8,1024,2,64]{1,3,2,0:T(8,128)(2,1)} %bitcast.79), kind=kOutput, calls=%fused_computation.35 | convolution fusion | flops 9109504 | bytes 2703392 | tf_op jit(solution)/shard_map/sgrd,slgd->sgrl/dot_general | solution.py:42
  59.5 0.8 reshape.157
  60.3 79.8 %reduce-window.6 = f32[8,2,4,8,128]{4,3,2,1,0:T(8,128)S(1)} reduce-window(f32[8,2,4,8,128]{4,3,2,1,0:T(8,128)} %reshape.157, f32[]{:T(128)} %constant.36.clone.1), window={size=1x1x1x1x128 pad=0_0x0_0x0_0x0_0x0_127}, to_apply=%region_1.2 | reduce-window | flops 8323072 | bytes 524292 | tf_op jit(solution)/shard_map/reduce-window
  140.1 0.4 copy.40
  140.6 1.3 reduce-window.9
  141.8 0.1 slice.11
  141.9 0.9 broadcast_add_fusion
  142.8 1.0 reduce_window_sum.26
  143.8 1.9 convolution_convert_fusion.3
  145.7 0.1 convert_element_type.82
  145.8 19.5 %all_gather.7 = bf16[128,512]{1,0:T(8,128)(2,1)S(1)} all-gather(bf16[8,512]{1,0:T(8,128)(2,1)S(1)} %convert_element_type.82), channel_id=1, replica_groups=mesh['grp'=2,'ep'=16] {'ep'}, dimensions={0}, use_global_device_ids=true | all-gather | bytes 139264 | tf_op jit(solution)/shard_map/all_gather | solution.py:87
  165.3 1.7 fusion.6
  167.0 3.6 %all-to-all-start = ((bf16[16,8,128]{2,1,0:T(8,128)(2,1)}), bf16[16,8,128]{2,1,0:T(8,128)(2,1)S(1)}, u32[]{:S(2)}, u32[]{:S(2)}) async-start(bf16[16,8,128]{2,1,0:T(8,128)(2,1)} %fusion.6), calls=%async_computation | async-start | bytes 65536 | tf_op jit(solution)/shard_map/all_to_all | solution.py:91
  170.6 0.1 convert_reduce_fusion
  170.7 6.5 %all-to-all-done = bf16[16,8,128]{2,1,0:T(8,128)(2,1)S(1)} async-done(((bf16[16,8,128]{2,1,0:T(8,128)(2,1)}), bf16[16,8,128]{2,1,0:T(8,128)(2,1)S(1)}, u32[]{:S(2)}, u32[]{:S(2)}) %all-to-all-start) | async-done | bytes 32800 | tf_op jit(solution)/shard_map/all_to_all | solution.py:91
  177.2 0.1 multiply_reduce_fusion.1
  177.3 0.3 convolution_convert_fusion.1
  177.7 0.9 reshape.161
  178.6 3.6 %all-to-all-start.1 = ((bf16[16,6,2048]{2,1,0:T(8,128)(2,1)}), bf16[16,6,2048]{2,1,0:T(8,128)(2,1)S(1)}, u32[]{:S(2)}, u32[]{:S(2)}) async-start(bf16[16,6,2048]{2,1,0:T(8,128)(2,1)} %reshape.161), calls=%async_computation.1 | async-start | bytes 1048576 | tf_op jit(solution)/shard_map/all_to_all | solution.py:115
  182.2 0.1 mul.105
  182.3 0.1 reduce_sum.64
  182.4 0.1 multiply_divide_fusion
  182.5 13.9 %all-to-all-done.1 = bf16[16,6,2048]{2,1,0:T(8,128)(2,1)S(1)} async-done(((bf16[16,6,2048]{2,1,0:T(8,128)(2,1)}), bf16[16,6,2048]{2,1,0:T(8,128)(2,1)S(1)}, u32[]{:S(2)}, u32[]{:S(2)}) %all-to-all-start.1) | async-done | bytes 393248 | tf_op jit(solution)/shard_map/all_to_all | solution.py:115
  196.4 1.6 convolution_bitcast_fusion.1
  198.0 0.0 copy-done
  198.1 0.0 copy-done.4
  198.1 0.8 convolution_convert_fusion
  198.8 0.0 copy-start.6
  198.9 1.0 copy.46
  199.9 4.1 %all-to-all-start.2 = ((bf16[16,6,2048]{2,1,0:T(8,128)(2,1)}), bf16[16,6,2048]{2,1,0:T(8,128)(2,1)S(1)}, u32[]{:S(2)}, u32[]{:S(2)}) async-start(bf16[16,6,2048]{2,1,0:T(8,128)(2,1)} %copy.46), calls=%async_computation.2 | async-start | bytes 1048576 | tf_op jit(solution)/shard_map/all_to_all | solution.py:123
  204.0 1.9 convolution_convert_fusion.5
  205.8 0.8 convolution_convert_fusion.6
  206.7 1.6 fusion.51
  208.2 10.0 %all-to-all-done.2 = bf16[16,6,2048]{2,1,0:T(8,128)(2,1)S(1)} async-done(((bf16[16,6,2048]{2,1,0:T(8,128)(2,1)}), bf16[16,6,2048]{2,1,0:T(8,128)(2,1)S(1)}, u32[]{:S(2)}, u32[]{:S(2)}) %all-to-all-start.2) | async-done | bytes 393248 | tf_op jit(solution)/shard_map/all_to_all | solution.py:123
  218.2 0.1 reshape.166
  218.4 0.7 gather_fusion
  219.1 0.1 gather.7
  219.1 0.3 multiply_reduce_fusion
  219.4 2.6 %fusion = bf16[8,2048]{1,0:T(8,128)(2,1)} fusion(bf16[256,2048]{1,0:T(8,128)(2,1)S(1)} %copy-done.5, bf16[2048,256]{1,0:T(8,128)(2,1)} %param.38, f32[8,2048]{1,0:T(8,128)S(1)} %multiply_reduce_fusion, bf16[16,8,128]{2,1,0:T(8,128)(2,1)S(1)} %all-to-all-done, bf16[8,2048]{1,0:T(8,128)(2,1)S(1)} %copy-done.1, f32[8,256]{1,0:T(8,128)S(1)} %fusion.51, ...), kind=kOutput, calls=%fused_computation.4 | convolution fusion | flops 16986112 | bytes 2277408 | tf_op jit(solution)/shard_map/dot_general | solution.py:20
  (21 shorter events, 0.1 us)
Async XLA Ops:
  7.2 190.9 %copy-start = (bf16[1,256,2048]{2,1,0:T(8,128)(2,1)S(1)}, bf16[1,256,2048]{2,1,0:T(8,128)(2,1)}, u32[]{:S(2)}) copy-start(bf16[1,256,2048]{2,1,0:T(8,128)(2,1)} %param.36) | copy-start | bytes 3145732
  7.2 47.2 %all-gather.2.cloned.1.call-start = ((), (), s32[]{:S(2)}) async-start(), calls=%async_computation.3 | async-start | bytes 2228224 | tf_op jit(solution)/shard_map/all_gather | solution.py:81
  8.6 4.1 %copy-start.11 = (f32[8]{0:T(128)S(1)}, f32[8]{0:T(128)}, u32[]{:S(2)}) copy-start(f32[8]{0:T(128)} %param.28) | copy-start | bytes 100
  8.6 4.2 %copy-start.2 = (bf16[8,1024,128]{2,1,0:T(8,128)(2,1)S(1)}, bf16[8,1024,128]{2,1,0:T(8,128)(2,1)}, u32[]{:S(2)}) copy-start(bf16[8,1024,128]{2,1,0:T(8,128)(2,1)} %param.27) | copy-start | bytes 6291460
  12.8 2.6 %copy-start.7 = (s32[8,6]{1,0:T(8,128)S(1)}, s32[8,6]{1,0:T(8,128)}, u32[]{:S(2)}) copy-start(s32[8,6]{1,0:T(8,128)} %param.32) | copy-start | bytes 580
  12.8 3.2 %copy-start.9 = (bf16[2048]{0:T(1024)(128)(2,1)S(1)}, bf16[2048]{0:T(1024)(128)(2,1)}, u32[]{:S(2)}) copy-start(bf16[2048]{0:T(1024)(128)(2,1)} %param.31) | copy-start | bytes 12292
  12.8 3.2 %copy-start.1 = (bf16[8,2048]{1,0:T(8,128)(2,1)S(1)}, bf16[8,2048]{1,0:T(8,128)(2,1)}, u32[]{:S(2)}) copy-start(bf16[8,2048]{1,0:T(8,128)(2,1)} %param.20) | copy-start | bytes 98308
  12.8 3.4 %copy-start.10 = (s32[8]{0:T(128)S(1)}, s32[8]{0:T(128)}, u32[]{:S(2)}) copy-start(s32[8]{0:T(128)} %param.30) | copy-start | bytes 100
  56.5 87.4 %copy-start.3 = (bf16[8,1024,128]{1,2,0:T(8,128)(2,1)S(1)}, bf16[8,1024,128]{1,2,0:T(8,128)(2,1)}, u32[]{:S(2)}) copy-start(bf16[8,1024,128]{1,2,0:T(8,128)(2,1)} %copy.42) | copy-start | bytes 6291460
  145.7 36.5 %copy-start.8 = (f32[8,6]{1,0:T(8,128)S(1)}, f32[8,6]{1,0:T(8,128)}, u32[]{:S(2)}) copy-start(f32[8,6]{1,0:T(8,128)} %param.33) | copy-start | bytes 580
  167.0 31.1 %copy-start.4 = (bf16[1,2048,256]{2,1,0:T(8,128)(2,1)S(1)}, bf16[1,2048,256]{2,1,0:T(8,128)(2,1)}, u32[]{:S(2)}) copy-start(bf16[1,2048,256]{2,1,0:T(8,128)(2,1)} %param.35) | copy-start | bytes 3145732
  167.0 10.2 %all-to-all-start = ((bf16[16,8,128]{2,1,0:T(8,128)(2,1)}), bf16[16,8,128]{2,1,0:T(8,128)(2,1)S(1)}, u32[]{:S(2)}, u32[]{:S(2)}) async-start(bf16[16,8,128]{2,1,0:T(8,128)(2,1)} %fusion.6), calls=%async_computation | async-start | bytes 65536 | tf_op jit(solution)/shard_map/all_to_all | solution.py:91
  178.6 17.8 %all-to-all-start.1 = ((bf16[16,6,2048]{2,1,0:T(8,128)(2,1)}), bf16[16,6,2048]{2,1,0:T(8,128)(2,1)S(1)}, u32[]{:S(2)}, u32[]{:S(2)}) async-start(bf16[16,6,2048]{2,1,0:T(8,128)(2,1)} %reshape.161), calls=%async_computation.1 | async-start | bytes 1048576 | tf_op jit(solution)/shard_map/all_to_all | solution.py:115
  198.8 7.0 %copy-start.6 = (bf16[2048,128]{1,0:T(8,128)(2,1)S(1)}, bf16[2048,128]{1,0:T(8,128)(2,1)}, u32[]{:S(2)}) copy-start(bf16[2048,128]{1,0:T(8,128)(2,1)} %param.23) | copy-start | bytes 1572868
  199.9 18.4 %all-to-all-start.2 = ((bf16[16,6,2048]{2,1,0:T(8,128)(2,1)}), bf16[16,6,2048]{2,1,0:T(8,128)(2,1)S(1)}, u32[]{:S(2)}, u32[]{:S(2)}) async-start(bf16[16,6,2048]{2,1,0:T(8,128)(2,1)} %copy.46), calls=%async_computation.2 | async-start | bytes 1048576 | tf_op jit(solution)/shard_map/all_to_all | solution.py:123
  206.7 12.8 %copy-start.5 = (bf16[256,2048]{1,0:T(8,128)(2,1)S(1)}, bf16[256,2048]{1,0:T(8,128)(2,1)}, u32[]{:S(2)}) copy-start(bf16[256,2048]{1,0:T(8,128)(2,1)} %param.39) | copy-start | bytes 3145732
Sparse Core Ops, SparseCore 0:
  10.1 44.1 all-gather.1
where the time goes:
time: 230 us; the launch traced here: 229 us
  other arithmetic  83.9 us (36%)
  waiting for transfers between devices  69.2 us (30%)
  blocking collectives  19.5 us (8%)
  matrix products  18.2 us (8%)
  between operations  14.2 us (6%)
  local copies, waits for them, and re-layouts  12.6 us (5%)
  starting transfers between devices  11.3 us (5%)
    another operation x2, other arithmetic  81.1 us
    all_gather x1, waiting for transfers between devices, shards(): lax.all_gather(w_query, 'ep', axis=0, tiled=True)  38.1 us
    all_gather x1, blocking collectives, shards(): lax.all_gather(attended, 'ep', axis=0, tiled=True)  19.5 us
    all_to_all x1, waiting for transfers between devices, shards(): lax.all_to_all(outgoing, 'ep', split_axis=0, concat_axis=0, tiled=True)  13.9 us
    all_to_all x1, waiting for transfers between devices, shards(): lax.all_to_all(result, 'ep', split_axis=0, concat_axis=0, tiled=True)  9.98 us
    unnamed x26, local copies, waits for them, and re-layouts  6.75 us
    all_to_all x1, waiting for transfers between devices, shards(): lax.all_to_all(out_columns, 'ep', split_axis=0, concat_axis=1, tiled=True)  6.52 us
  transfers between devices with their start and end apart: 4, of which 4 were waited for; matrix products, arithmetic and copies ran while one was open for 6% of the time, Pallas kernels for 0%

commit v1 on v0

--- a/solution.py
+++ b/solution.py
@@ -6,6 +6,28 @@
 
 EPSILON = 1e-06
 ROUTED_SCALE = 2.5
+
+
+def cut_along(array, dim, size):
+    before, after = (array.shape[:dim], array.shape[dim + 1 :])
+    return jnp.moveaxis(array.reshape(*before, size, -1, *after), dim, 0)
+
+
+def joined_along(blocks, dim):
+    shape = list(blocks.shape[1:])
+    shape[dim] *= blocks.shape[0]
+    return jnp.moveaxis(blocks, 0, dim).reshape(shape)
+
+
+def swapped_with_each(value, axis, split_dim, concat_dim):
+    size, index = (lax.axis_size(axis), lax.axis_index(axis))
+    blocks = cut_along(value, split_dim, size)
+    outs = [blocks[index]]
+    for step in range(1, size):
+        sent = blocks[index ^ step]
+        outs.append(lax.ppermute(sent, axis, [(i, i ^ step) for i in range(size)]))
+    blocks = jnp.stack(outs)[index ^ jnp.arange(size)]
+    return joined_along(blocks, concat_dim)
 
 
 def norm_rows(values, gain_vec):
@@ -120,7 +142,7 @@
     hidden = (jax.nn.silu(gate_part) * up_part).astype(jnp.bfloat16)
     result = jnp.einsum("sekf,efd->sekd", hidden, w_down, preferred_element_type=jnp.float32)
     result = result.astype(jnp.bfloat16).reshape(devices * local_count, slot_count, model_width)
-    returned = lax.all_to_all(result, "ep", split_axis=0, concat_axis=0, tiled=True)
+    returned = swapped_with_each(result, "ep", 0, 0)
     returned_rows = returned.reshape(experts_all * capacity, model_width)
     picked = jnp.take(returned_rows, slot_place, axis=0).reshape(seq_dev, top_count, model_width)
     routed = jnp.sum(picked.astype(jnp.float32) * route_share[:, :, None], axis=1)

time: 230 us -> 240 us (1.043)
  starting transfers between devices: 11.3 us -> 27.9 us
  waiting for transfers between devices: 69.2 us -> 58.7 us
  local copies, waits for them, and re-layouts: 12.6 us -> 15.5 us
    ppermute x0 -> x15, starting transfers between devices: none -> 20.8 us  [swapped_with_each(): outs.append(lax.ppermute(sent, axis, [(i, i ^ step) for i in range(size)]))]
    all_to_all x1 -> x0, waiting for transfers between devices: 9.98 us -> none  [shards(): lax.all_to_all(result, 'ep', split_axis=0, concat_axis=0, tiled=True)]
    all_to_all x1, waiting for transfers between devices: 13.9 us -> 8.83 us  [shards(): lax.all_to_all(outgoing, 'ep', split_axis=0, concat_axis=0, tiled=True)]
    ppermute x0 -> x15, waiting for transfers between devices: none -> 4.88 us  [swapped_with_each(): outs.append(lax.ppermute(sent, axis, [(i, i ^ step) for i in range(size)]))]
    all_to_all x1 -> x0, starting transfers between devices: 4.09 us -> none  [shards(): lax.all_to_all(result, 'ep', split_axis=0, concat_axis=0, tiled=True)]
    unnamed x26 -> x56, local copies, waits for them, and re-layouts: 6.75 us -> 7.86 us
  transfers between devices with their start and end apart: 4 -> 18, of which waited for: 4 -> 5; matrix products, arithmetic and copies ran while one was open for 6% -> 6% of each run, Pallas kernels for 0% -> 0%
where the time goes in v1:
time: 240 us; the launch traced here: 239 us
  other arithmetic  83.9 us (35%)
  waiting for transfers between devices  58.7 us (24%)
  starting transfers between devices  27.9 us (12%)
  blocking collectives  19.5 us (8%)
  matrix products  19.2 us (8%)
  local copies, waits for them, and re-layouts  15.5 us (6%)
  between operations  14.5 us (6%)
    another operation x2, other arithmetic  81.1 us
    all_gather x1, waiting for transfers between devices, shards(): lax.all_gather(w_query, 'ep', axis=0, tiled=True)  37.8 us
    ppermute x15, starting transfers between devices, swapped_with_each(): outs.append(lax.ppermute(sent, axis, [(i, i ^ step) for i in range(size)]))  20.8 us
    all_gather x1, blocking collectives, shards(): lax.all_gather(attended, 'ep', axis=0, tiled=True)  19.5 us
    all_to_all x1, waiting for transfers between devices, shards(): lax.all_to_all(outgoing, 'ep', split_axis=0, concat_axis=0, tiled=True)  8.83 us
    unnamed x56, local copies, waits for them, and re-layouts  7.86 us
    all_to_all x1, waiting for transfers between devices, shards(): lax.all_to_all(out_columns, 'ep', split_axis=0, concat_axis=1, tiled=True)  6.58 us
    ppermute x15, waiting for transfers between devices, swapped_with_each(): outs.append(lax.ppermute(sent, axis, [(i, i ^ step) for i in range(size)]))  4.88 us
  transfers between devices with their start and end apart: 18, of which 5 were waited for; matrix products, arithmetic and copies ran while one was open for 6% of the time, Pallas kernels for 0%

profile of v1, /device:TPU:0, one launch (start us, length us, event | category | flops | bytes accessed | tf_op | source)
XLA Modules:
  0.0 239.2 jit_solution(14597139561668581975)
XLA Ops:
  7.2 0.7 all-gather.2.cloned.1.call-update
  7.9 0.7 convert_element_type.77
  8.6 4.1 %copy.382 = bf16[8,1024,128]{1,2,0:T(8,128)(2,1)} copy(bf16[8,1024,128]{2,1,0:T(8,128)(2,1)} %param.26) | data formatting | bytes 4194304 | tf_op args[6]
  12.7 0.1 add.160
  12.8 2.6 %copy.385 = bf16[8,1024,128]{1,2,0:T(8,128)(2,1)} copy(bf16[8,1024,128]{2,1,0:T(8,128)(2,1)S(1)} %copy-done.2) | data formatting | bytes 4194304 | tf_op args[7]
  15.4 0.1 reshape.220
  15.6 0.2 select_reduce_fusion
  15.8 0.1 reduce_sum.60
  15.9 0.1 copy.386
  16.0 0.1 mul.105
  16.1 0.1 reduce_sum.64
  16.2 0.1 convert_reduce_fusion
  16.3 0.1 fusion.31
  16.5 0.1 iota_compare_fusion
  16.6 37.8 %all-gather.2.cloned.1.call-done = bf16[2048,512]{1,0:T(8,128)(2,1)} async-done(((bf16[128,512]{1,0:T(8,128)(2,1)}), bf16[2048,512]{1,0:T(8,128)(2,1)}) %all-gather.2.cloned.1.call-update) | async-done | bytes 2097168 | tf_op jit(solution)/shard_map/all_gather | solution.py:103
  54.4 2.0 convolution_convert_fusion.4
  56.4 0.1 reshape.215
  56.5 3.0 %fusion.22 = (f32[8,2,4,1024]{3,2,1,0:T(4,128)S(1)}, f32[8,2,4,1024]{3,2,1,0:T(4,128)}) fusion(pred[8,1024]{1,0:T(8,128)(4,1)S(1)} %iota_compare_fusion, f32[8,2,1024]{2,1,0:T(2,128)} %param.29, f32[2,4]{1,0:T(2,128)S(1)} %add.160, bf16[8,2,4,64]{3,2,1,0:T(4,128)(2,1)S(1)} %reshape.215, bf16[8,1024,2,64]{1,3,2,0:T(8,128)(2,1)} %bitcast.283), kind=kOutput, calls=%fused_computation.36 | convolution fusion | flops 9109504 | bytes 2703392 | tf_op jit(solution)/shard_map/sgrd,slgd->sgrl/dot_general | solution.py:64
  59.5 0.8 reshape.217
  60.3 79.8 %reduce-window.6 = f32[8,2,4,8,128]{4,3,2,1,0:T(8,128)S(1)} reduce-window(f32[8,2,4,8,128]{4,3,2,1,0:T(8,128)} %reshape.217, f32[]{:T(128)} %constant.27.clone.1), window={size=1x1x1x1x128 pad=0_0x0_0x0_0x0_0x0_127}, to_apply=%region_1.2 | reduce-window | flops 8323072 | bytes 524292 | tf_op jit(solution)/shard_map/reduce-window
  140.1 0.4 copy.383
  140.5 1.3 reduce-window.9
  141.9 0.8 broadcast_add_fusion
  142.7 1.0 reduce_window_sum.26
  143.8 1.9 convolution_convert_fusion.3
  145.7 0.1 convert_element_type.82
  145.8 19.5 %all_gather.7 = bf16[128,512]{1,0:T(8,128)(2,1)S(1)} all-gather(bf16[8,512]{1,0:T(8,128)(2,1)S(1)} %convert_element_type.82), channel_id=1, replica_groups=mesh['grp'=2,'ep'=16] {'ep'}, dimensions={0}, use_global_device_ids=true | all-gather | bytes 139264 | tf_op jit(solution)/shard_map/all_gather | solution.py:109
  165.2 1.7 fusion.6
  166.9 3.5 %all-to-all-start = ((bf16[16,8,128]{2,1,0:T(8,128)(2,1)}), bf16[16,8,128]{2,1,0:T(8,128)(2,1)S(1)}, u32[]{:S(2)}, u32[]{:S(2)}) async-start(bf16[16,8,128]{2,1,0:T(8,128)(2,1)} %fusion.6), calls=%async_computation | async-start | bytes 65536 | tf_op jit(solution)/shard_map/all_to_all | solution.py:113
  170.4 6.6 %all-to-all-done = bf16[16,8,128]{2,1,0:T(8,128)(2,1)S(1)} async-done(((bf16[16,8,128]{2,1,0:T(8,128)(2,1)}), bf16[16,8,128]{2,1,0:T(8,128)(2,1)S(1)}, u32[]{:S(2)}, u32[]{:S(2)}) %all-to-all-start) | async-done | bytes 32800 | tf_op jit(solution)/shard_map/all_to_all | solution.py:113
  177.0 0.1 multiply_reduce_fusion.1
  177.1 0.3 convolution_convert_fusion.1
  177.5 0.9 reshape.221
  178.4 3.6 %all-to-all-start.1 = ((bf16[16,6,2048]{2,1,0:T(8,128)(2,1)}), bf16[16,6,2048]{2,1,0:T(8,128)(2,1)S(1)}, u32[]{:S(2)}, u32[]{:S(2)}) async-start(bf16[16,6,2048]{2,1,0:T(8,128)(2,1)} %reshape.221), calls=%async_computation.1 | async-start | bytes 1048576 | tf_op jit(solution)/shard_map/all_to_all | solution.py:137
  182.1 1.9 convolution_convert_fusion.5
  184.0 1.9 convolution_convert_fusion.6
  185.9 1.5 fusion.52
  187.4 8.8 %all-to-all-done.1 = bf16[16,6,2048]{2,1,0:T(8,128)(2,1)S(1)} async-done(((bf16[16,6,2048]{2,1,0:T(8,128)(2,1)}), bf16[16,6,2048]{2,1,0:T(8,128)(2,1)S(1)}, u32[]{:S(2)}, u32[]{:S(2)}) %all-to-all-start.1) | async-done | bytes 393248 | tf_op jit(solution)/shard_map/all_to_all | solution.py:137
  196.2 1.6 convolution_bitcast_fusion.1
  197.9 0.8 convolution_convert_fusion
  198.7 1.2 dynamic-slice_bitcast_fusion
  199.9 0.2 collective-permute-start
  200.1 1.3 collective-permute-start.1
  201.4 0.5 collective-permute-start.2
  202.0 1.4 collective-permute-start.3
  203.5 0.5 collective-permute-start.4
  204.2 2.1 collective-permute-start.5
  206.4 0.5 collective-permute-start.6
  206.9 2.4 collective-permute-start.7
  209.3 0.3 collective-permute-start.8
  209.6 1.8 collective-permute-start.9
  211.4 1.7 collective-permute-start.10
  213.1 1.8 collective-permute-start.11
  215.0 1.7 collective-permute-start.12
  216.7 3.0 %collective-permute-start.13 = (bf16[1,6,2048]{2,1,0:T(8,128)(2,1)S(1)}, bf16[1,6,2048]{2,1,0:T(8,128)(2,1)S(1)}, u32[]{:S(2)}, u32[]{:S(2)}) collective-permute-start(bf16[1,6,2048]{2,1,0:T(8,128)(2,1)S(1)} %bitcast.287), channel_id=1, source_target_pairs={{0,14},{1,15},{2,12},{3,13},{4,10},{5,11},{6,8},{7,9},{8,6},{9,7},... | collective-permute-start | bytes 73736 | tf_op jit(solution)/shard_map/ppermute | solution.py:28
  219.7 1.5 collective-permute-start.14
  221.2 2.1 collective-permute-done.13
  223.3 2.7 %collective-permute-done.14 = bf16[1,6,2048]{2,1,0:T(8,128)(2,1)S(1)} collective-permute-done((bf16[1,6,2048]{2,1,0:T(8,128)(2,1)S(1)}, bf16[1,6,2048]{2,1,0:T(8,128)(2,1)S(1)}, u32[]{:S(2)}, u32[]{:S(2)}) %collective-permute-start.14) | collective-permute-done | bytes 24608 | tf_op jit(solution)/shard_map/ppermute | solution.py:28
  226.0 0.8 copy-done.6
  226.8 1.7 gather_fusion
  228.6 0.1 reshape_reshape.3
  228.7 0.7 gather_fusion.1
  229.5 0.3 multiply_reduce_fusion
  229.8 2.6 %fusion = bf16[8,2048]{1,0:T(8,128)(2,1)} fusion(bf16[256,2048]{1,0:T(8,128)(2,1)S(1)} %copy-done.5, bf16[2048,256]{1,0:T(8,128)(2,1)} %param.38, f32[8,2048]{1,0:T(8,128)S(1)} %multiply_reduce_fusion, bf16[16,8,128]{2,1,0:T(8,128)(2,1)S(1)} %all-to-all-done, bf16[8,2048]{1,0:T(8,128)(2,1)S(1)} %copy-done.1, f32[8,256]{1,0:T(8,128)S(1)} %fusion.52, ...), kind=kOutput, calls=%fused_computation.5 | convolution fusion | flops 16986112 | bytes 2277408 | tf_op jit(solution)/shard_map/dot_general | solution.py:42
  (83 shorter events, 0.9 us)
Async XLA Ops:
  7.2 190.7 %copy-start = (bf16[1,256,2048]{2,1,0:T(8,128)(2,1)S(1)}, bf16[1,256,2048]{2,1,0:T(8,128)(2,1)}, u32[]{:S(2)}) copy-start(bf16[1,256,2048]{2,1,0:T(8,128)(2,1)} %param.36) | copy-start | bytes 3145732
  7.2 47.2 %all-gather.2.cloned.1.call-start = ((), (), s32[]{:S(2)}) async-start(), calls=%async_computation.2 | async-start | bytes 2228224 | tf_op jit(solution)/shard_map/all_gather | solution.py:103
  8.6 4.1 %copy-start.11 = (f32[8]{0:T(128)S(1)}, f32[8]{0:T(128)}, u32[]{:S(2)}) copy-start(f32[8]{0:T(128)} %param.28) | copy-start | bytes 100
  8.6 4.1 %copy-start.2 = (bf16[8,1024,128]{2,1,0:T(8,128)(2,1)S(1)}, bf16[8,1024,128]{2,1,0:T(8,128)(2,1)}, u32[]{:S(2)}) copy-start(bf16[8,1024,128]{2,1,0:T(8,128)(2,1)} %param.27) | copy-start | bytes 6291460
  12.8 2.6 %copy-start.7 = (s32[8,6]{1,0:T(8,128)S(1)}, s32[8,6]{1,0:T(8,128)}, u32[]{:S(2)}) copy-start(s32[8,6]{1,0:T(8,128)} %param.32) | copy-start | bytes 580
  12.8 3.2 %copy-start.9 = (bf16[2048]{0:T(1024)(128)(2,1)S(1)}, bf16[2048]{0:T(1024)(128)(2,1)}, u32[]{:S(2)}) copy-start(bf16[2048]{0:T(1024)(128)(2,1)} %param.31) | copy-start | bytes 12292
  12.8 3.3 %copy-start.8 = (f32[8,6]{1,0:T(8,128)S(1)}, f32[8,6]{1,0:T(8,128)}, u32[]{:S(2)}) copy-start(f32[8,6]{1,0:T(8,128)} %param.33) | copy-start | bytes 580
  12.8 3.5 %copy-start.1 = (bf16[8,2048]{1,0:T(8,128)(2,1)S(1)}, bf16[8,2048]{1,0:T(8,128)(2,1)}, u32[]{:S(2)}) copy-start(bf16[8,2048]{1,0:T(8,128)(2,1)} %param.20) | copy-start | bytes 98308
  12.8 3.7 %copy-start.10 = (s32[8]{0:T(128)S(1)}, s32[8]{0:T(128)}, u32[]{:S(2)}) copy-start(s32[8]{0:T(128)} %param.30) | copy-start | bytes 100
  56.5 87.3 %copy-start.3 = (bf16[8,1024,128]{1,2,0:T(8,128)(2,1)S(1)}, bf16[8,1024,128]{1,2,0:T(8,128)(2,1)}, u32[]{:S(2)}) copy-start(bf16[8,1024,128]{1,2,0:T(8,128)(2,1)} %copy.385) | copy-start | bytes 6291460
  166.9 10.1 %all-to-all-start = ((bf16[16,8,128]{2,1,0:T(8,128)(2,1)}), bf16[16,8,128]{2,1,0:T(8,128)(2,1)S(1)}, u32[]{:S(2)}, u32[]{:S(2)}) async-start(bf16[16,8,128]{2,1,0:T(8,128)(2,1)} %fusion.6), calls=%async_computation | async-start | bytes 65536 | tf_op jit(solution)/shard_map/all_to_all | solution.py:113
  178.4 17.8 %all-to-all-start.1 = ((bf16[16,6,2048]{2,1,0:T(8,128)(2,1)}), bf16[16,6,2048]{2,1,0:T(8,128)(2,1)S(1)}, u32[]{:S(2)}, u32[]{:S(2)}) async-start(bf16[16,6,2048]{2,1,0:T(8,128)(2,1)} %reshape.221), calls=%async_computation.1 | async-start | bytes 1048576 | tf_op jit(solution)/shard_map/all_to_all | solution.py:137
  182.0 15.9 %copy-start.4 = (bf16[1,2048,256]{2,1,0:T(8,128)(2,1)S(1)}, bf16[1,2048,256]{2,1,0:T(8,128)(2,1)}, u32[]{:S(2)}) copy-start(bf16[1,2048,256]{2,1,0:T(8,128)(2,1)} %param.35) | copy-start | bytes 3145732
  199.9 4.3 %collective-permute-start = (bf16[1,6,2048]{2,1,0:T(8,128)(2,1)S(1)}, bf16[1,6,2048]{2,1,0:T(8,128)(2,1)S(1)}, u32[]{:S(2)}, u32[]{:S(2)}) collective-permute-start(bf16[1,6,2048]{2,1,0:T(8,128)(2,1)S(1)} %bitcast.300), channel_id=1, source_target_pairs={{0,1},{1,0},{2,3},{3,2},{4,5},{5,4},{6,7},{7,6},{8,9},{9,8},{10,11... | collective-permute-start | bytes 73736 | tf_op jit(solution)/shard_map/ppermute | solution.py:28
  200.1 6.3 %collective-permute-start.1 = (bf16[1,6,2048]{2,1,0:T(8,128)(2,1)S(1)}, bf16[1,6,2048]{2,1,0:T(8,128)(2,1)S(1)}, u32[]{:S(2)}, u32[]{:S(2)}) collective-permute-start(bf16[1,6,2048]{2,1,0:T(8,128)(2,1)S(1)} %bitcast.299), channel_id=1, source_target_pairs={{0,2},{1,3},{2,0},{3,1},{4,6},{5,7},{6,4},{7,5},{8,10},{9,11},{10,... | collective-permute-start | bytes 73736 | tf_op jit(solution)/shard_map/ppermute | solution.py:28
  201.4 5.5 %collective-permute-start.2 = (bf16[1,6,2048]{2,1,0:T(8,128)(2,1)S(1)}, bf16[1,6,2048]{2,1,0:T(8,128)(2,1)S(1)}, u32[]{:S(2)}, u32[]{:S(2)}) collective-permute-start(bf16[1,6,2048]{2,1,0:T(8,128)(2,1)S(1)} %bitcast.298), channel_id=1, source_target_pairs={{0,3},{1,2},{2,1},{3,0},{4,7},{5,6},{6,5},{7,4},{8,11},{9,10},{10,... | collective-permute-start | bytes 73736 | tf_op jit(solution)/shard_map/ppermute | solution.py:28
  202.0 7.3 %collective-permute-start.3 = (bf16[1,6,2048]{2,1,0:T(8,128)(2,1)S(1)}, bf16[1,6,2048]{2,1,0:T(8,128)(2,1)S(1)}, u32[]{:S(2)}, u32[]{:S(2)}) collective-permute-start(bf16[1,6,2048]{2,1,0:T(8,128)(2,1)S(1)} %bitcast.297), channel_id=1, source_target_pairs={{0,4},{1,5},{2,6},{3,7},{4,0},{5,1},{6,2},{7,3},{8,12},{9,13},{10,... | collective-permute-start | bytes 73736 | tf_op jit(solution)/shard_map/ppermute | solution.py:28
  203.5 6.1 %collective-permute-start.4 = (bf16[1,6,2048]{2,1,0:T(8,128)(2,1)S(1)}, bf16[1,6,2048]{2,1,0:T(8,128)(2,1)S(1)}, u32[]{:S(2)}, u32[]{:S(2)}) collective-permute-start(bf16[1,6,2048]{2,1,0:T(8,128)(2,1)S(1)} %bitcast.296), channel_id=1, source_target_pairs={{0,5},{1,4},{2,7},{3,6},{4,1},{5,0},{6,3},{7,2},{8,13},{9,12},{10,... | collective-permute-start | bytes 73736 | tf_op jit(solution)/shard_map/ppermute | solution.py:28
  204.2 7.2 %collective-permute-start.5 = (bf16[1,6,2048]{2,1,0:T(8,128)(2,1)S(1)}, bf16[1,6,2048]{2,1,0:T(8,128)(2,1)S(1)}, u32[]{:S(2)}, u32[]{:S(2)}) collective-permute-start(bf16[1,6,2048]{2,1,0:T(8,128)(2,1)S(1)} %bitcast.295), channel_id=1, source_target_pairs={{0,6},{1,7},{2,4},{3,5},{4,2},{5,3},{6,0},{7,1},{8,14},{9,15},{10,... | collective-permute-start | bytes 73736 | tf_op jit(solution)/shard_map/ppermute | solution.py:28
  206.4 6.8 %collective-permute-start.6 = (bf16[1,6,2048]{2,1,0:T(8,128)(2,1)S(1)}, bf16[1,6,2048]{2,1,0:T(8,128)(2,1)S(1)}, u32[]{:S(2)}, u32[]{:S(2)}) collective-permute-start(bf16[1,6,2048]{2,1,0:T(8,128)(2,1)S(1)} %bitcast.294), channel_id=1, source_target_pairs={{0,7},{1,6},{2,5},{3,4},{4,3},{5,2},{6,1},{7,0},{8,15},{9,14},{10,... | collective-permute-start | bytes 73736 | tf_op jit(solution)/shard_map/ppermute | solution.py:28
  206.9 8.1 %collective-permute-start.7 = (bf16[1,6,2048]{2,1,0:T(8,128)(2,1)S(1)}, bf16[1,6,2048]{2,1,0:T(8,128)(2,1)S(1)}, u32[]{:S(2)}, u32[]{:S(2)}) collective-permute-start(bf16[1,6,2048]{2,1,0:T(8,128)(2,1)S(1)} %bitcast.293), channel_id=1, source_target_pairs={{0,8},{1,9},{2,10},{3,11},{4,12},{5,13},{6,14},{7,15},{8,0},{9,1},... | collective-permute-start | bytes 73736 | tf_op jit(solution)/shard_map/ppermute | solution.py:28
  209.3 7.4 %collective-permute-start.8 = (bf16[1,6,2048]{2,1,0:T(8,128)(2,1)S(1)}, bf16[1,6,2048]{2,1,0:T(8,128)(2,1)S(1)}, u32[]{:S(2)}, u32[]{:S(2)}) collective-permute-start(bf16[1,6,2048]{2,1,0:T(8,128)(2,1)S(1)} %bitcast.292), channel_id=1, source_target_pairs={{0,9},{1,8},{2,11},{3,10},{4,13},{5,12},{6,15},{7,14},{8,1},{9,0},... | collective-permute-start | bytes 73736 | tf_op jit(solution)/shard_map/ppermute | solution.py:28
  209.6 10.1 %collective-permute-start.9 = (bf16[1,6,2048]{2,1,0:T(8,128)(2,1)S(1)}, bf16[1,6,2048]{2,1,0:T(8,128)(2,1)S(1)}, u32[]{:S(2)}, u32[]{:S(2)}) collective-permute-start(bf16[1,6,2048]{2,1,0:T(8,128)(2,1)S(1)} %bitcast.291), channel_id=1, source_target_pairs={{0,10},{1,11},{2,8},{3,9},{4,14},{5,15},{6,12},{7,13},{8,2},{9,3},... | collective-permute-start | bytes 73736 | tf_op jit(solution)/shard_map/ppermute | solution.py:28
  211.4 9.7 %collective-permute-start.10 = (bf16[1,6,2048]{2,1,0:T(8,128)(2,1)S(1)}, bf16[1,6,2048]{2,1,0:T(8,128)(2,1)S(1)}, u32[]{:S(2)}, u32[]{:S(2)}) collective-permute-start(bf16[1,6,2048]{2,1,0:T(8,128)(2,1)S(1)} %bitcast.290), channel_id=1, source_target_pairs={{0,11},{1,10},{2,9},{3,8},{4,15},{5,14},{6,13},{7,12},{8,3},{9,2},... | collective-permute-start | bytes 73736 | tf_op jit(solution)/shard_map/ppermute | solution.py:28
  213.1 8.0 %collective-permute-start.11 = (bf16[1,6,2048]{2,1,0:T(8,128)(2,1)S(1)}, bf16[1,6,2048]{2,1,0:T(8,128)(2,1)S(1)}, u32[]{:S(2)}, u32[]{:S(2)}) collective-permute-start(bf16[1,6,2048]{2,1,0:T(8,128)(2,1)S(1)} %bitcast.289), channel_id=1, source_target_pairs={{0,12},{1,13},{2,14},{3,15},{4,8},{5,9},{6,10},{7,11},{8,4},{9,5},... | collective-permute-start | bytes 73736 | tf_op jit(solution)/shard_map/ppermute | solution.py:28
  215.0 6.2 %collective-permute-start.12 = (bf16[1,6,2048]{2,1,0:T(8,128)(2,1)S(1)}, bf16[1,6,2048]{2,1,0:T(8,128)(2,1)S(1)}, u32[]{:S(2)}, u32[]{:S(2)}) collective-permute-start(bf16[1,6,2048]{2,1,0:T(8,128)(2,1)S(1)} %bitcast.288), channel_id=1, source_target_pairs={{0,13},{1,12},{2,15},{3,14},{4,9},{5,8},{6,11},{7,10},{8,5},{9,4},... | collective-permute-start | bytes 73736 | tf_op jit(solution)/shard_map/ppermute | solution.py:28
  216.7 6.6 %collective-permute-start.13 = (bf16[1,6,2048]{2,1,0:T(8,128)(2,1)S(1)}, bf16[1,6,2048]{2,1,0:T(8,128)(2,1)S(1)}, u32[]{:S(2)}, u32[]{:S(2)}) collective-permute-start(bf16[1,6,2048]{2,1,0:T(8,128)(2,1)S(1)} %bitcast.287), channel_id=1, source_target_pairs={{0,14},{1,15},{2,12},{3,13},{4,10},{5,11},{6,8},{7,9},{8,6},{9,7},... | collective-permute-start | bytes 73736 | tf_op jit(solution)/shard_map/ppermute | solution.py:28
  219.7 6.4 %collective-permute-start.14 = (bf16[1,6,2048]{2,1,0:T(8,128)(2,1)S(1)}, bf16[1,6,2048]{2,1,0:T(8,128)(2,1)S(1)}, u32[]{:S(2)}, u32[]{:S(2)}) collective-permute-start(bf16[1,6,2048]{2,1,0:T(8,128)(2,1)S(1)} %bitcast.286), channel_id=1, source_target_pairs={{0,15},{1,14},{2,13},{3,12},{4,11},{5,10},{6,9},{7,8},{8,7},{9,6},... | collective-permute-start | bytes 73736 | tf_op jit(solution)/shard_map/ppermute | solution.py:28
  226.0 0.8 copy-start.6
  226.8 2.9 %copy-start.5 = (bf16[256,2048]{1,0:T(8,128)(2,1)S(1)}, bf16[256,2048]{1,0:T(8,128)(2,1)}, u32[]{:S(2)}) copy-start(bf16[256,2048]{1,0:T(8,128)(2,1)} %param.39) | copy-start | bytes 3145732
Sparse Core Ops, SparseCore 0:
  10.1 44.1 all-gather.1
